TPU v7x, 32 devices: a whole 2x2x4 slice. The times are simulated.
32 devices in a mesh: pp: 4 (over z), fs: 4 (over y, x), tp: 2 (over core).
Axes of the slice: x: 2, y: 2, z: 4, core: 2. Of those that a mesh axis runs over, the one named last changes fastest.
Arguments:
- tokens: bfloat16 [4, 512, 1024], P('pp', 'fs', 'tp'), parts along dimension 1, may hold values from -640 to 640
- query_matrix: bfloat16 [4, 1024, 1024], P('pp', None, 'tp'), may hold values from -0.1875 to 0.1875
- key_matrix: bfloat16 [4, 1024, 1024], P('pp', None, 'tp'), may hold values from -0.1875 to 0.1875
- value_matrix: bfloat16 [4, 1024, 1024], P('pp', None, 'tp'), may hold values from -0.1875 to 0.1875
- output_gate_weight: bfloat16 [4, 1024, 1024], P('pp', None, 'tp'), may hold values from -0.1875 to 0.1875
- strength_weight: bfloat16 [4, 1024, 8], P('pp', None, 'tp'), may hold values from -0.1875 to 0.1875
- decay_input_weight: bfloat16 [4, 1024, 8], P('pp', None, 'tp'), may hold values from -0.1875 to 0.1875
- decay_scale_table: float32 [4, 8], P('pp', 'tp'), may hold values from 0.00078125 to 0.234375
- log_spike_decay: float32 [4, 128, 8], P('pp', None, 'tp'), may hold values from -2.1 to 0
- head_norm_gain: float32 [4, 1024], P('pp', 'tp'), may hold values from 0.1 to 1.9
- closing_norm_gain: float32 [1024], P('tp'), may hold values from 0.1 to 1.9
Outputs:
- normalized: bfloat16 [4, 512, 1024], P('pp', 'fs', 'tp'), parts along dimension 1
There are 4 independent parts, one for each index of `fs`. A program takes and returns all parts, laid end to end along the dimension named above; an argument that names none is the same for every part. Nothing has to cross between parts.
All inputs are finite; a program needn't handle non-finite values.
Results may differ from a plain program's by a relative error of at most 0.012.
Values may be sent and summed in bfloat16 or wider, within the bound.
A program may use at most 64 MiB of HBM per device.

v0:
```python
import jax
import jax.numpy as jnp
from jax import lax
from jax.sharding import PartitionSpec as P

BLOCK = 64


epsilon = 1e-06


def from_behind(block, axis, distance):
    devices = range(lax.axis_size(axis))
    route = [((i - distance) % len(devices), i) for i in devices]
    return lax.ppermute(block, axis, route)


def unit_lower_inverse(system):
    best_precision = lax.Precision.HIGHEST
    leading = system.shape[:-2]
    lead_count = len(leading)
    order = system.shape[-1]
    inverse = jnp.ones(leading + (order, 1, 1), jnp.float32)
    span = 1
    while span < order:
        count = order // (2 * span)
        tiles = system.reshape(leading + (count, 2 * span, count, 2 * span))
        diagonal_tiles = jnp.diagonal(tiles, axis1=lead_count, axis2=lead_count + 2)
        diagonal_tiles = jnp.moveaxis(diagonal_tiles, -1, lead_count)
        lower_left = diagonal_tiles[..., span:, :span]
        paired = inverse.reshape(leading + (count, 2, span, span))
        first = paired[..., 0, :, :]
        second = paired[..., 1, :, :]
        partial_left = jnp.einsum("...ij,...jk->...ik", lower_left, first, precision=best_precision)
        corner = -jnp.einsum("...ij,...jk->...ik", second, partial_left, precision=best_precision)
        top = jnp.concatenate([first, jnp.zeros_like(first)], axis=-1)
        bottom = jnp.concatenate([corner, second], axis=-1)
        inverse = jnp.concatenate([top, bottom], axis=-2)
        span = span * 2
    return inverse[..., 0, :, :]


def delta_rule(queries, keys_unit, values, beta_gate, decay_logarithm):
    length, head_count, head_width = queries.shape
    value_width = values.shape[-1]
    num_blocks = length // BLOCK
    best_precision = lax.Precision.HIGHEST

    def to_blocks(tensor):
        return tensor.reshape(num_blocks, BLOCK, head_count, -1).transpose(2, 0, 1, 3)

    query_b = to_blocks(queries)
    keys_b = to_blocks(keys_unit)
    values_b = to_blocks(values)
    beta_b = beta_gate.reshape(num_blocks, BLOCK, head_count).transpose(2, 0, 1)
    decay_b = decay_logarithm.reshape(num_blocks, BLOCK, head_count).transpose(2, 0, 1)
    cumulative = jnp.cumsum(decay_b, axis=-1)
    row_ids = lax.broadcasted_iota(jnp.int32, (BLOCK, BLOCK), 0)
    col_ids = lax.broadcasted_iota(jnp.int32, (BLOCK, BLOCK), 1)
    within = jnp.where(
        row_ids >= col_ids, cumulative[..., :, None] - cumulative[..., None, :], -jnp.inf
    )
    weights = jnp.exp(within)
    keys_beta = keys_b * beta_b[..., None]
    self_term = jnp.where(
        row_ids > col_ids,
        jnp.einsum("hnik,hnjk->hnij", keys_beta, keys_b, precision=best_precision) * weights,
        0.0,
    )
    system = self_term + jnp.eye(BLOCK, dtype=self_term.dtype)
    right_side = jnp.concatenate(
        [values_b * beta_b[..., None], keys_beta * jnp.exp(cumulative)[..., None]], axis=-1
    )
    inverse = unit_lower_inverse(system)
    solved = jnp.einsum("hnij,hnjc->hnic", inverse, right_side, precision=best_precision)
    update = solved[..., :value_width]
    correct = solved[..., value_width:]
    scores = jnp.einsum("hnik,hnjk->hnij", query_b, keys_b, precision=best_precision) * weights
    query_dec = query_b * jnp.exp(cumulative)[..., None]
    keys_dec = keys_b * jnp.exp(cumulative[..., -1:] - cumulative)[..., None]
    block_decay = jnp.exp(cumulative[..., -1])

    def advance(state_matrix, inputs):
        (
            state_update,
            correction_term,
            normed_queries,
            normed_keys,
            attention_scores,
            decay_factor,
        ) = inputs
        new_state = state_update - jnp.einsum(
            "rna,raq->rnq", correction_term, state_matrix, precision=best_precision
        )
        normed_output = jnp.einsum(
            "rna,raq->rnq", normed_queries, state_matrix, precision=best_precision
        ) + jnp.einsum("pak,pkr->par", attention_scores, new_state, precision=best_precision)
        state_matrix = state_matrix * decay_factor[:, None, None] + jnp.einsum(
            "fni,fnl->fil", normed_keys, new_state, precision=best_precision
        )
        return (state_matrix, normed_output)

    sequence_in = tuple(
        (
            jnp.moveaxis(tensor, 1, 0)
            for tensor in (update, correct, query_dec, keys_dec, scores, block_decay)
        )
    )
    initial_state = jnp.zeros((head_count, head_width, value_width), jnp.float32)
    final_state, outputs = lax.scan(advance, initial_state, sequence_in)
    return outputs.transpose(0, 2, 1, 3).reshape(length, head_count, value_width)


def merge_head_outputs(
    query_projected,
    key_projected,
    value_projected,
    gate_logits,
    strength_logits,
    decay_logits,
    decay_speed,
    spike_log_values,
    gain_vector,
):
    length = query_projected.shape[0]
    head_count = strength_logits.shape[-1]
    head_width = query_projected.shape[1] // head_count

    def normalize(projected):
        activated = jax.nn.silu(projected).reshape(length, head_count, -1)
        return activated * lax.rsqrt(
            jnp.sum(activated * activated, axis=-1, keepdims=True) + epsilon
        )

    queries = normalize(query_projected) * head_width ** (-0.5)
    keys_unit = normalize(key_projected)
    values = jax.nn.silu(value_projected).reshape(length, head_count, -1)
    beta_gate = jax.nn.sigmoid(strength_logits)
    decay_logarithm = -decay_speed[None, :] * jax.nn.softplus(decay_logits) + spike_log_values
    mixed_out = delta_rule(queries, keys_unit, values, beta_gate, decay_logarithm)
    mixed_out = (
        mixed_out
        * lax.rsqrt(jnp.mean(mixed_out * mixed_out, axis=-1, keepdims=True) + epsilon)
        * gain_vector.reshape(head_count, -1)
        * jax.nn.silu(gate_logits).reshape(length, head_count, -1)
    )
    return mixed_out.reshape(length, -1).astype(jnp.bfloat16)


def on_device(
    tokens,
    query_matrix,
    key_matrix,
    value_matrix,
    output_gate_weight,
    strength_weight,
    decay_input_weight,
    decay_scale_table,
    log_spike_decay,
    head_norm_gain,
    closing_norm_gain,
):
    section_count = lax.axis_size("pp")
    position = lax.axis_index("pp")
    matrices = (
        query_matrix[0],
        key_matrix[0],
        value_matrix[0],
        output_gate_weight[0],
        strength_weight[0],
        decay_input_weight[0],
    )
    decay_speed = decay_scale_table[0]
    spike_log_values = log_spike_decay[0]
    gain_vector = head_norm_gain[0]
    model_width = matrices[0].shape[0]
    row_count = tokens.shape[1]

    def is_active(step_index):
        offset = step_index - position
        return (offset >= 0) & (offset < section_count)

    def heads_of(projected):
        return merge_head_outputs(
            projected[0],
            projected[1],
            projected[2],
            projected[3],
            projected[4],
            projected[5],
            decay_speed,
            spike_log_values,
            gain_vector,
        )

    def advance_columns(step_index, carried):
        arriving = from_behind(carried, "pp", 1)
        initial = tuple(
            (jnp.zeros((row_count, matrix.shape[1]), jnp.float32) for matrix in matrices)
        )
        initial = initial + (jnp.zeros((row_count, 1), jnp.float32),)
        piece = lax.all_gather(arriving, "tp", axis=1, tiled=True)
        square = piece.astype(jnp.float32)
        sums = tuple(
            (jnp.dot(piece, matrix, preferred_element_type=jnp.float32) for matrix in matrices)
        )
        totals = sums + (jnp.sum(square * square, axis=1, keepdims=True),)
        inv_rms = lax.rsqrt(totals[-1] / model_width + epsilon)
        projected = [total * inv_rms for total in totals[:-1]]
        head_out = heads_of(projected)
        updated = (arriving.astype(jnp.float32) + head_out.astype(jnp.float32)).astype(jnp.bfloat16)
        return jnp.where(is_active(step_index), updated, arriving)

    own_columns = lax.fori_loop(0, 2 * section_count - 1, advance_columns, tokens[0])
    placed = from_behind(own_columns, "pp", 1)
    square = placed.astype(jnp.float32)
    row_total = lax.psum(jnp.sum(square * square, axis=1), "tp")
    inv_rms = lax.rsqrt(row_total / model_width + epsilon)[:, None]
    normalized = (square * inv_rms * closing_norm_gain[None, :]).astype(jnp.bfloat16)
    return normalized[None]


def solution(mesh):
    placed = (
        P("pp", "fs", "tp"),
        P("pp", None, "tp"),
        P("pp", None, "tp"),
        P("pp", None, "tp"),
        P("pp", None, "tp"),
        P("pp", None, "tp"),
        P("pp", None, "tp"),
        P("pp", "tp"),
        P("pp", None, "tp"),
        P("pp", "tp"),
        P("tp"),
    )
    return jax.shard_map(
        on_device, mesh=mesh, in_specs=placed, out_specs=P("pp", "fs", "tp"), check_vma=False
    )
```

profile of v0, /device:TPU:0, one launch (start us, length us, event | category | flops | bytes accessed | tf_op | source)
XLA Modules:
  0.0 532.5 jit_solution(3828281167846604389)
XLA Ops:
  1.6 519.5 %while.47 = (s32[]{:T(128)}, bf16[128,512]{1,0:T(8,128)(2,1)S(1)}, s32[]{:T(128)}, bf16[1024,512]{1,0:T(8,128)(2,1)}, bf16[1024,4]{0,1:T(4,128)(2,1)}, /*index=5...) while((s32[]{:T(128)}, bf16[128,512]{1,0:T(8,128)(2,1)S(1)}, ...), condition=%wide.region_8.9_spmd, body=%wide.region_0.8_spmd.sunk | while | flops 929622144 | bytes 34070800 | solution.py:214
  1.6 3.1 collective-permute-start
  5.9 4.3 collective-permute-done
  17.4 2.8 copy.394
  20.2 3.6 reshape.402
  28.9 4.8 copy.395
  33.7 2.9 gather_fusion
  38.1 6.2 %copy.399 = f32[4,2,16,4,16,4]{5,3,4,2,1,0:T(4,128)} copy(f32[4,2,16,4,16,4]{5,4,3,2,1,0:T(8,128)} %reshape.402) | data formatting | bytes 262144 | tf_op jit(solution)/shard_map/while/body/eval_jaxpr/reshape | solution.py:27
  44.3 3.6 gather_fusion.1
  57.0 2.2 gather_fusion.2
  71.1 3.3 while.48
  78.1 6.1 %collective-permute-done = bf16[128,512]{1,0:T(8,128)(2,1)S(1)} collective-permute-done((bf16[128,512]{1,0:T(8,128)(2,1)S(1)}, bf16[128,512]{1,0:T(8,128)(2,1)S(1)}, u32[]{:S(2)}, u32[]{:S(2)}) %collective-permute-start) | collective-permute-done | bytes 131104 | tf_op jit(solution)/shard_map/while/body/eval_jaxpr/ppermute | solution.py:15
  91.4 2.8 copy.394
  94.3 3.6 reshape.402
  103.0 4.8 copy.395
  107.8 2.9 gather_fusion
  112.2 6.2 %copy.399 = f32[4,2,16,4,16,4]{5,3,4,2,1,0:T(4,128)} copy(f32[4,2,16,4,16,4]{5,4,3,2,1,0:T(8,128)} %reshape.402) | data formatting | bytes 262144 | tf_op jit(solution)/shard_map/while/body/eval_jaxpr/reshape | solution.py:27
  118.4 3.6 gather_fusion.1
  131.1 2.2 gather_fusion.2
  145.2 3.3 while.48
  152.2 6.1 %collective-permute-done = bf16[128,512]{1,0:T(8,128)(2,1)S(1)} collective-permute-done((bf16[128,512]{1,0:T(8,128)(2,1)S(1)}, bf16[128,512]{1,0:T(8,128)(2,1)S(1)}, u32[]{:S(2)}, u32[]{:S(2)}) %collective-permute-start) | collective-permute-done | bytes 131104 | tf_op jit(solution)/shard_map/while/body/eval_jaxpr/ppermute | solution.py:15
  165.5 2.8 copy.394
  168.3 3.6 reshape.402
  177.0 4.8 copy.395
  181.8 2.9 gather_fusion
  186.2 6.2 %copy.399 = f32[4,2,16,4,16,4]{5,3,4,2,1,0:T(4,128)} copy(f32[4,2,16,4,16,4]{5,4,3,2,1,0:T(8,128)} %reshape.402) | data formatting | bytes 262144 | tf_op jit(solution)/shard_map/while/body/eval_jaxpr/reshape | solution.py:27
  192.4 3.6 gather_fusion.1
  205.2 2.2 gather_fusion.2
  219.2 3.3 while.48
  226.2 6.1 %collective-permute-done = bf16[128,512]{1,0:T(8,128)(2,1)S(1)} collective-permute-done((bf16[128,512]{1,0:T(8,128)(2,1)S(1)}, bf16[128,512]{1,0:T(8,128)(2,1)S(1)}, u32[]{:S(2)}, u32[]{:S(2)}) %collective-permute-start) | collective-permute-done | bytes 131104 | tf_op jit(solution)/shard_map/while/body/eval_jaxpr/ppermute | solution.py:15
  239.5 2.8 copy.394
  242.4 3.6 reshape.402
  251.1 4.8 copy.395
  255.9 2.9 gather_fusion
  260.3 6.2 %copy.399 = f32[4,2,16,4,16,4]{5,3,4,2,1,0:T(4,128)} copy(f32[4,2,16,4,16,4]{5,4,3,2,1,0:T(8,128)} %reshape.402) | data formatting | bytes 262144 | tf_op jit(solution)/shard_map/while/body/eval_jaxpr/reshape | solution.py:27
  266.5 3.6 gather_fusion.1
  279.2 2.2 gather_fusion.2
  293.3 3.3 while.48
  300.3 6.1 %collective-permute-done = bf16[128,512]{1,0:T(8,128)(2,1)S(1)} collective-permute-done((bf16[128,512]{1,0:T(8,128)(2,1)S(1)}, bf16[128,512]{1,0:T(8,128)(2,1)S(1)}, u32[]{:S(2)}, u32[]{:S(2)}) %collective-permute-start) | collective-permute-done | bytes 131104 | tf_op jit(solution)/shard_map/while/body/eval_jaxpr/ppermute | solution.py:15
  313.6 2.8 copy.394
  316.4 3.6 reshape.402
  325.1 4.8 copy.395
  329.9 2.9 gather_fusion
  334.3 6.2 %copy.399 = f32[4,2,16,4,16,4]{5,3,4,2,1,0:T(4,128)} copy(f32[4,2,16,4,16,4]{5,4,3,2,1,0:T(8,128)} %reshape.402) | data formatting | bytes 262144 | tf_op jit(solution)/shard_map/while/body/eval_jaxpr/reshape | solution.py:27
  340.5 3.6 gather_fusion.1
  367.3 3.3 while.48
  374.3 6.1 %collective-permute-done = bf16[128,512]{1,0:T(8,128)(2,1)S(1)} collective-permute-done((bf16[128,512]{1,0:T(8,128)(2,1)S(1)}, bf16[128,512]{1,0:T(8,128)(2,1)S(1)}, u32[]{:S(2)}, u32[]{:S(2)}) %collective-permute-start) | collective-permute-done | bytes 131104 | tf_op jit(solution)/shard_map/while/body/eval_jaxpr/ppermute | solution.py:15
  387.7 2.8 copy.394
  390.5 3.6 reshape.402
  399.2 4.8 copy.395
  404.0 2.9 gather_fusion
  408.4 6.2 %copy.399 = f32[4,2,16,4,16,4]{5,3,4,2,1,0:T(4,128)} copy(f32[4,2,16,4,16,4]{5,4,3,2,1,0:T(8,128)} %reshape.402) | data formatting | bytes 262144 | tf_op jit(solution)/shard_map/while/body/eval_jaxpr/reshape | solution.py:27
  414.6 3.6 gather_fusion.1
  441.4 3.3 while.48
  448.4 6.1 %collective-permute-done = bf16[128,512]{1,0:T(8,128)(2,1)S(1)} collective-permute-done((bf16[128,512]{1,0:T(8,128)(2,1)S(1)}, bf16[128,512]{1,0:T(8,128)(2,1)S(1)}, u32[]{:S(2)}, u32[]{:S(2)}) %collective-permute-start) | collective-permute-done | bytes 131104 | tf_op jit(solution)/shard_map/while/body/eval_jaxpr/ppermute | solution.py:15
  461.7 2.8 copy.394
  464.5 3.6 reshape.402
  473.3 4.8 copy.395
  478.0 2.9 gather_fusion
  482.4 6.2 %copy.399 = f32[4,2,16,4,16,4]{5,3,4,2,1,0:T(4,128)} copy(f32[4,2,16,4,16,4]{5,4,3,2,1,0:T(8,128)} %reshape.402) | data formatting | bytes 262144 | tf_op jit(solution)/shard_map/while/body/eval_jaxpr/reshape | solution.py:27
  488.7 3.6 gather_fusion.1
  515.4 3.3 while.48
  521.2 7.3 %collective-permute-done.1 = bf16[128,512]{1,0:T(8,128)(2,1)S(1)} collective-permute-done((bf16[128,512]{1,0:T(8,128)(2,1)S(1)}, bf16[128,512]{1,0:T(8,128)(2,1)S(1)}, u32[]{:S(2)}, u32[]{:S(2)}) %collective-permute-start.1) | collective-permute-done | bytes 131104 | tf_op jit(solution)/shard_map/ppermute | solution.py:15
  528.6 2.5 psum.7
  (988 shorter events, 296.4 us)
Async XLA Ops:
  1.6 18.6 %copy-start.17 = (f32[1,4]{1,0:T(1,128)}, f32[1,4]{1,0:T(1,128)S(1)}, u32[]{:S(2)}) copy-start(f32[1,4]{1,0:T(1,128)S(1)} %get-tuple-element.754) | copy-start | bytes 52 | tf_op jit(solution)/shard_map/while
  1.6 14.8 %copy-start.9 = (bf16[1024,4]{0,1:T(4,128)(2,1)S(1)}, bf16[1024,4]{0,1:T(4,128)(2,1)}, u32[]{:S(2)}) copy-start(bf16[1024,4]{0,1:T(4,128)(2,1)} %get-tuple-element.753) | copy-start | bytes 24580 | tf_op jit(solution)/shard_map/while
  1.6 8.6 %collective-permute-start = (bf16[128,512]{1,0:T(8,128)(2,1)S(1)}, bf16[128,512]{1,0:T(8,128)(2,1)S(1)}, u32[]{:S(2)}, u32[]{:S(2)}) collective-permute-start(bf16[128,512]{1,0:T(8,128)(2,1)S(1)} %get-tuple-element.731), channel_id=1, source_target_pairs={{24,0},{0,8},{8,16},{16,24},{25,1},{1,9},{9,17},{17,25},{26,2},{2,... | collective-permute-start | bytes 393224 | tf_op jit(solution)/shard_map/while/body/eval_jaxpr/ppermute | solution.py:15
  4.6 15.6 %copy-start.10 = (pred[64,64]{1,0:T(8,128)(4,1)}, pred[64,64]{1,0:T(8,128)(4,1)S(1)}, u32[]{:S(2)}) copy-start(pred[64,64]{1,0:T(8,128)(4,1)S(1)} %get-tuple-element.650) | copy-start | bytes 12292 | tf_op jit(solution)/shard_map/while
  12.3 7.9 %copy-start.13 = (f32[128]{0:T(128)}, f32[128]{0:T(128)S(1)}, u32[]{:S(2)}) copy-start(f32[128]{0:T(128)S(1)} %add_rsqrt_fusion.9) | copy-start | bytes 1540 | tf_op jit(solution)/shard_map/while
  28.9 7.8 %copy-start.5 = (f32[4,2,32,1,2]{0,4,3,1,2:T(2,128)S(1)}, f32[4,2,32,1,2]{0,4,3,1,2:T(2,128)}, u32[]{:S(2)}) copy-start(f32[4,2,32,1,2]{0,4,3,1,2:T(2,128)} %get-tuple-element.764) | copy-start | bytes 6148 | tf_op jit(solution)/shard_map/while
  59.2 4.9 copy-start
  59.9 4.3 copy-start.12
  71.1 5.6 %copy-start.18 = (f32[1,4]{1,0:T(1,128)S(1)}, f32[1,4]{1,0:T(1,128)}, u32[]{:S(2)}) copy-start(f32[1,4]{1,0:T(1,128)} %copy-done.17) | copy-start | bytes 52 | tf_op jit(solution)/shard_map/while
  76.8 17.5 %copy-start.17 = (f32[1,4]{1,0:T(1,128)}, f32[1,4]{1,0:T(1,128)S(1)}, u32[]{:S(2)}) copy-start(f32[1,4]{1,0:T(1,128)S(1)} %get-tuple-element.754) | copy-start | bytes 52 | tf_op jit(solution)/shard_map/while
  76.8 13.6 %copy-start.9 = (bf16[1024,4]{0,1:T(4,128)(2,1)S(1)}, bf16[1024,4]{0,1:T(4,128)(2,1)}, u32[]{:S(2)}) copy-start(bf16[1024,4]{0,1:T(4,128)(2,1)} %get-tuple-element.753) | copy-start | bytes 24580 | tf_op jit(solution)/shard_map/while
  76.8 7.4 %collective-permute-start = (bf16[128,512]{1,0:T(8,128)(2,1)S(1)}, bf16[128,512]{1,0:T(8,128)(2,1)S(1)}, u32[]{:S(2)}, u32[]{:S(2)}) collective-permute-start(bf16[128,512]{1,0:T(8,128)(2,1)S(1)} %get-tuple-element.731), channel_id=1, source_target_pairs={{24,0},{0,8},{8,16},{16,24},{25,1},{1,9},{9,17},{17,25},{26,2},{2,... | collective-permute-start | bytes 393224 | tf_op jit(solution)/shard_map/while/body/eval_jaxpr/ppermute | solution.py:15
  76.9 17.4 %copy-start.10 = (pred[64,64]{1,0:T(8,128)(4,1)}, pred[64,64]{1,0:T(8,128)(4,1)S(1)}, u32[]{:S(2)}) copy-start(pred[64,64]{1,0:T(8,128)(4,1)S(1)} %get-tuple-element.650) | copy-start | bytes 12292 | tf_op jit(solution)/shard_map/while
  86.3 7.9 %copy-start.13 = (f32[128]{0:T(128)}, f32[128]{0:T(128)S(1)}, u32[]{:S(2)}) copy-start(f32[128]{0:T(128)S(1)} %add_rsqrt_fusion.9) | copy-start | bytes 1540 | tf_op jit(solution)/shard_map/while
  103.0 7.8 %copy-start.5 = (f32[4,2,32,1,2]{0,4,3,1,2:T(2,128)S(1)}, f32[4,2,32,1,2]{0,4,3,1,2:T(2,128)}, u32[]{:S(2)}) copy-start(f32[4,2,32,1,2]{0,4,3,1,2:T(2,128)} %get-tuple-element.764) | copy-start | bytes 6148 | tf_op jit(solution)/shard_map/while
  133.3 4.9 copy-start
  133.9 4.3 copy-start.12
  145.2 5.6 %copy-start.18 = (f32[1,4]{1,0:T(1,128)S(1)}, f32[1,4]{1,0:T(1,128)}, u32[]{:S(2)}) copy-start(f32[1,4]{1,0:T(1,128)} %copy-done.17) | copy-start | bytes 52 | tf_op jit(solution)/shard_map/while
  150.8 17.5 %copy-start.17 = (f32[1,4]{1,0:T(1,128)}, f32[1,4]{1,0:T(1,128)S(1)}, u32[]{:S(2)}) copy-start(f32[1,4]{1,0:T(1,128)S(1)} %get-tuple-element.754) | copy-start | bytes 52 | tf_op jit(solution)/shard_map/while
  150.8 13.6 %copy-start.9 = (bf16[1024,4]{0,1:T(4,128)(2,1)S(1)}, bf16[1024,4]{0,1:T(4,128)(2,1)}, u32[]{:S(2)}) copy-start(bf16[1024,4]{0,1:T(4,128)(2,1)} %get-tuple-element.753) | copy-start | bytes 24580 | tf_op jit(solution)/shard_map/while
  150.8 7.4 %collective-permute-start = (bf16[128,512]{1,0:T(8,128)(2,1)S(1)}, bf16[128,512]{1,0:T(8,128)(2,1)S(1)}, u32[]{:S(2)}, u32[]{:S(2)}) collective-permute-start(bf16[128,512]{1,0:T(8,128)(2,1)S(1)} %get-tuple-element.731), channel_id=1, source_target_pairs={{24,0},{0,8},{8,16},{16,24},{25,1},{1,9},{9,17},{17,25},{26,2},{2,... | collective-permute-start | bytes 393224 | tf_op jit(solution)/shard_map/while/body/eval_jaxpr/ppermute | solution.py:15
  150.9 17.4 %copy-start.10 = (pred[64,64]{1,0:T(8,128)(4,1)}, pred[64,64]{1,0:T(8,128)(4,1)S(1)}, u32[]{:S(2)}) copy-start(pred[64,64]{1,0:T(8,128)(4,1)S(1)} %get-tuple-element.650) | copy-start | bytes 12292 | tf_op jit(solution)/shard_map/while
  160.4 7.9 %copy-start.13 = (f32[128]{0:T(128)}, f32[128]{0:T(128)S(1)}, u32[]{:S(2)}) copy-start(f32[128]{0:T(128)S(1)} %add_rsqrt_fusion.9) | copy-start | bytes 1540 | tf_op jit(solution)/shard_map/while
  177.0 7.8 %copy-start.5 = (f32[4,2,32,1,2]{0,4,3,1,2:T(2,128)S(1)}, f32[4,2,32,1,2]{0,4,3,1,2:T(2,128)}, u32[]{:S(2)}) copy-start(f32[4,2,32,1,2]{0,4,3,1,2:T(2,128)} %get-tuple-element.764) | copy-start | bytes 6148 | tf_op jit(solution)/shard_map/while
  207.4 4.9 copy-start
  208.0 4.3 copy-start.12
  219.2 5.6 %copy-start.18 = (f32[1,4]{1,0:T(1,128)S(1)}, f32[1,4]{1,0:T(1,128)}, u32[]{:S(2)}) copy-start(f32[1,4]{1,0:T(1,128)} %copy-done.17) | copy-start | bytes 52 | tf_op jit(solution)/shard_map/while
  224.9 17.5 %copy-start.17 = (f32[1,4]{1,0:T(1,128)}, f32[1,4]{1,0:T(1,128)S(1)}, u32[]{:S(2)}) copy-start(f32[1,4]{1,0:T(1,128)S(1)} %get-tuple-element.754) | copy-start | bytes 52 | tf_op jit(solution)/shard_map/while
  224.9 13.6 %copy-start.9 = (bf16[1024,4]{0,1:T(4,128)(2,1)S(1)}, bf16[1024,4]{0,1:T(4,128)(2,1)}, u32[]{:S(2)}) copy-start(bf16[1024,4]{0,1:T(4,128)(2,1)} %get-tuple-element.753) | copy-start | bytes 24580 | tf_op jit(solution)/shard_map/while
  224.9 7.4 %collective-permute-start = (bf16[128,512]{1,0:T(8,128)(2,1)S(1)}, bf16[128,512]{1,0:T(8,128)(2,1)S(1)}, u32[]{:S(2)}, u32[]{:S(2)}) collective-permute-start(bf16[128,512]{1,0:T(8,128)(2,1)S(1)} %get-tuple-element.731), channel_id=1, source_target_pairs={{24,0},{0,8},{8,16},{16,24},{25,1},{1,9},{9,17},{17,25},{26,2},{2,... | collective-permute-start | bytes 393224 | tf_op jit(solution)/shard_map/while/body/eval_jaxpr/ppermute | solution.py:15
  225.0 17.4 %copy-start.10 = (pred[64,64]{1,0:T(8,128)(4,1)}, pred[64,64]{1,0:T(8,128)(4,1)S(1)}, u32[]{:S(2)}) copy-start(pred[64,64]{1,0:T(8,128)(4,1)S(1)} %get-tuple-element.650) | copy-start | bytes 12292 | tf_op jit(solution)/shard_map/while
  234.4 7.9 %copy-start.13 = (f32[128]{0:T(128)}, f32[128]{0:T(128)S(1)}, u32[]{:S(2)}) copy-start(f32[128]{0:T(128)S(1)} %add_rsqrt_fusion.9) | copy-start | bytes 1540 | tf_op jit(solution)/shard_map/while
  251.1 7.8 %copy-start.5 = (f32[4,2,32,1,2]{0,4,3,1,2:T(2,128)S(1)}, f32[4,2,32,1,2]{0,4,3,1,2:T(2,128)}, u32[]{:S(2)}) copy-start(f32[4,2,32,1,2]{0,4,3,1,2:T(2,128)} %get-tuple-element.764) | copy-start | bytes 6148 | tf_op jit(solution)/shard_map/while
  281.4 4.9 copy-start
  282.0 4.3 copy-start.12
  293.3 5.6 %copy-start.18 = (f32[1,4]{1,0:T(1,128)S(1)}, f32[1,4]{1,0:T(1,128)}, u32[]{:S(2)}) copy-start(f32[1,4]{1,0:T(1,128)} %copy-done.17) | copy-start | bytes 52 | tf_op jit(solution)/shard_map/while
  298.9 17.5 %copy-start.17 = (f32[1,4]{1,0:T(1,128)}, f32[1,4]{1,0:T(1,128)S(1)}, u32[]{:S(2)}) copy-start(f32[1,4]{1,0:T(1,128)S(1)} %get-tuple-element.754) | copy-start | bytes 52 | tf_op jit(solution)/shard_map/while
  298.9 13.6 %copy-start.9 = (bf16[1024,4]{0,1:T(4,128)(2,1)S(1)}, bf16[1024,4]{0,1:T(4,128)(2,1)}, u32[]{:S(2)}) copy-start(bf16[1024,4]{0,1:T(4,128)(2,1)} %get-tuple-element.753) | copy-start | bytes 24580 | tf_op jit(solution)/shard_map/while
  299.0 7.4 %collective-permute-start = (bf16[128,512]{1,0:T(8,128)(2,1)S(1)}, bf16[128,512]{1,0:T(8,128)(2,1)S(1)}, u32[]{:S(2)}, u32[]{:S(2)}) collective-permute-start(bf16[128,512]{1,0:T(8,128)(2,1)S(1)} %get-tuple-element.731), channel_id=1, source_target_pairs={{24,0},{0,8},{8,16},{16,24},{25,1},{1,9},{9,17},{17,25},{26,2},{2,... | collective-permute-start | bytes 393224 | tf_op jit(solution)/shard_map/while/body/eval_jaxpr/ppermute | solution.py:15
  299.0 17.4 %copy-start.10 = (pred[64,64]{1,0:T(8,128)(4,1)}, pred[64,64]{1,0:T(8,128)(4,1)S(1)}, u32[]{:S(2)}) copy-start(pred[64,64]{1,0:T(8,128)(4,1)S(1)} %get-tuple-element.650) | copy-start | bytes 12292 | tf_op jit(solution)/shard_map/while
  308.5 7.9 %copy-start.13 = (f32[128]{0:T(128)}, f32[128]{0:T(128)S(1)}, u32[]{:S(2)}) copy-start(f32[128]{0:T(128)S(1)} %add_rsqrt_fusion.9) | copy-start | bytes 1540 | tf_op jit(solution)/shard_map/while
  325.1 7.8 %copy-start.5 = (f32[4,2,32,1,2]{0,4,3,1,2:T(2,128)S(1)}, f32[4,2,32,1,2]{0,4,3,1,2:T(2,128)}, u32[]{:S(2)}) copy-start(f32[4,2,32,1,2]{0,4,3,1,2:T(2,128)} %get-tuple-element.764) | copy-start | bytes 6148 | tf_op jit(solution)/shard_map/while
  355.5 4.9 copy-start
  356.1 4.3 copy-start.12
  367.3 5.6 %copy-start.18 = (f32[1,4]{1,0:T(1,128)S(1)}, f32[1,4]{1,0:T(1,128)}, u32[]{:S(2)}) copy-start(f32[1,4]{1,0:T(1,128)} %copy-done.17) | copy-start | bytes 52 | tf_op jit(solution)/shard_map/while
  373.0 17.5 %copy-start.17 = (f32[1,4]{1,0:T(1,128)}, f32[1,4]{1,0:T(1,128)S(1)}, u32[]{:S(2)}) copy-start(f32[1,4]{1,0:T(1,128)S(1)} %get-tuple-element.754) | copy-start | bytes 52 | tf_op jit(solution)/shard_map/while
  373.0 13.6 %copy-start.9 = (bf16[1024,4]{0,1:T(4,128)(2,1)S(1)}, bf16[1024,4]{0,1:T(4,128)(2,1)}, u32[]{:S(2)}) copy-start(bf16[1024,4]{0,1:T(4,128)(2,1)} %get-tuple-element.753) | copy-start | bytes 24580 | tf_op jit(solution)/shard_map/while
  373.0 7.4 %collective-permute-start = (bf16[128,512]{1,0:T(8,128)(2,1)S(1)}, bf16[128,512]{1,0:T(8,128)(2,1)S(1)}, u32[]{:S(2)}, u32[]{:S(2)}) collective-permute-start(bf16[128,512]{1,0:T(8,128)(2,1)S(1)} %get-tuple-element.731), channel_id=1, source_target_pairs={{24,0},{0,8},{8,16},{16,24},{25,1},{1,9},{9,17},{17,25},{26,2},{2,... | collective-permute-start | bytes 393224 | tf_op jit(solution)/shard_map/while/body/eval_jaxpr/ppermute | solution.py:15
  373.1 17.4 %copy-start.10 = (pred[64,64]{1,0:T(8,128)(4,1)}, pred[64,64]{1,0:T(8,128)(4,1)S(1)}, u32[]{:S(2)}) copy-start(pred[64,64]{1,0:T(8,128)(4,1)S(1)} %get-tuple-element.650) | copy-start | bytes 12292 | tf_op jit(solution)/shard_map/while
  382.5 7.9 %copy-start.13 = (f32[128]{0:T(128)}, f32[128]{0:T(128)S(1)}, u32[]{:S(2)}) copy-start(f32[128]{0:T(128)S(1)} %add_rsqrt_fusion.9) | copy-start | bytes 1540 | tf_op jit(solution)/shard_map/while
  399.2 7.8 %copy-start.5 = (f32[4,2,32,1,2]{0,4,3,1,2:T(2,128)S(1)}, f32[4,2,32,1,2]{0,4,3,1,2:T(2,128)}, u32[]{:S(2)}) copy-start(f32[4,2,32,1,2]{0,4,3,1,2:T(2,128)} %get-tuple-element.764) | copy-start | bytes 6148 | tf_op jit(solution)/shard_map/while
  429.5 4.9 copy-start
  430.1 4.3 copy-start.12
  441.4 5.6 %copy-start.18 = (f32[1,4]{1,0:T(1,128)S(1)}, f32[1,4]{1,0:T(1,128)}, u32[]{:S(2)}) copy-start(f32[1,4]{1,0:T(1,128)} %copy-done.17) | copy-start | bytes 52 | tf_op jit(solution)/shard_map/while
  447.0 17.5 %copy-start.17 = (f32[1,4]{1,0:T(1,128)}, f32[1,4]{1,0:T(1,128)S(1)}, u32[]{:S(2)}) copy-start(f32[1,4]{1,0:T(1,128)S(1)} %get-tuple-element.754) | copy-start | bytes 52 | tf_op jit(solution)/shard_map/while
  447.1 13.6 %copy-start.9 = (bf16[1024,4]{0,1:T(4,128)(2,1)S(1)}, bf16[1024,4]{0,1:T(4,128)(2,1)}, u32[]{:S(2)}) copy-start(bf16[1024,4]{0,1:T(4,128)(2,1)} %get-tuple-element.753) | copy-start | bytes 24580 | tf_op jit(solution)/shard_map/while
  447.1 7.4 %collective-permute-start = (bf16[128,512]{1,0:T(8,128)(2,1)S(1)}, bf16[128,512]{1,0:T(8,128)(2,1)S(1)}, u32[]{:S(2)}, u32[]{:S(2)}) collective-permute-start(bf16[128,512]{1,0:T(8,128)(2,1)S(1)} %get-tuple-element.731), channel_id=1, source_target_pairs={{24,0},{0,8},{8,16},{16,24},{25,1},{1,9},{9,17},{17,25},{26,2},{2,... | collective-permute-start | bytes 393224 | tf_op jit(solution)/shard_map/while/body/eval_jaxpr/ppermute | solution.py:15
  447.2 17.4 %copy-start.10 = (pred[64,64]{1,0:T(8,128)(4,1)}, pred[64,64]{1,0:T(8,128)(4,1)S(1)}, u32[]{:S(2)}) copy-start(pred[64,64]{1,0:T(8,128)(4,1)S(1)} %get-tuple-element.650) | copy-start | bytes 12292 | tf_op jit(solution)/shard_map/while
  456.6 7.9 %copy-start.13 = (f32[128]{0:T(128)}, f32[128]{0:T(128)S(1)}, u32[]{:S(2)}) copy-start(f32[128]{0:T(128)S(1)} %add_rsqrt_fusion.9) | copy-start | bytes 1540 | tf_op jit(solution)/shard_map/while
  473.3 7.8 %copy-start.5 = (f32[4,2,32,1,2]{0,4,3,1,2:T(2,128)S(1)}, f32[4,2,32,1,2]{0,4,3,1,2:T(2,128)}, u32[]{:S(2)}) copy-start(f32[4,2,32,1,2]{0,4,3,1,2:T(2,128)} %get-tuple-element.764) | copy-start | bytes 6148 | tf_op jit(solution)/shard_map/while
  503.6 4.9 copy-start
  504.2 4.3 copy-start.12
  515.4 5.6 %copy-start.18 = (f32[1,4]{1,0:T(1,128)S(1)}, f32[1,4]{1,0:T(1,128)}, u32[]{:S(2)}) copy-start(f32[1,4]{1,0:T(1,128)} %copy-done.17) | copy-start | bytes 52 | tf_op jit(solution)/shard_map/while
  521.1 7.4 %collective-permute-start.1 = (bf16[128,512]{1,0:T(8,128)(2,1)S(1)}, bf16[128,512]{1,0:T(8,128)(2,1)S(1)}, u32[]{:S(2)}, u32[]{:S(2)}) collective-permute-start(bf16[128,512]{1,0:T(8,128)(2,1)S(1)} %get-tuple-element.327), channel_id=1, source_target_pairs={{24,0},{0,8},{8,16},{16,24},{25,1},{1,9},{9,17},{17,25},{26,2},{2,... | collective-permute-start | bytes 393224 | tf_op jit(solution)/shard_map/ppermute | solution.py:15
  (77 other events, 217.2 us)
where the time goes:
time: 536 us; the launch traced here: 533 us
  local copies, waits for them, and re-layouts  300 us (56%)
  matrix products  120 us (22%)
  waiting for transfers between devices  48.1 us (9%)
  other arithmetic  39.1 us (7%)
  blocking collectives  16.3 us (3%)
  loops' own time  6.04 us (1%)
    reshape x63, local copies, waits for them, and re-layouts, unit_lower_inverse(): tiles = system.reshape(leading + (count, 2 * span, count, 2 * span))  147 us
    gather x63, local copies, waits for them, and re-layouts, unit_lower_inverse(): diagonal_tiles = jnp.diagonal(tiles, axis1=lead_count, axis2=lead_count + 2)  77.1 us
    ppermute x8, waiting for transfers between devices, from_behind(): return lax.ppermute(block, axis, route)  48.1 us
    dot_general x42, matrix products, advance_columns(): jnp.dot(piece, matrix, preferred_element_type=jnp.float32)  43.5 us
    while x294, local copies, waits for them, and re-layouts  24 us
    dot_general x35, matrix products, unit_lower_inverse(): jnp.einsum('...ij,...jk->...ik', second, partial_left, precision=best_pre...  22.9 us
    add x7, local copies, waits for them, and re-layouts, delta_rule(): system = self_term + jnp.eye(BLOCK, dtype=self_term.dtype)  19.8 us
    dot_general x35, matrix products, unit_lower_inverse(): jnp.einsum('...ij,...jk->...ik', lower_left, first, precision=best_precis...  16.8 us
  transfers between devices with their start and end apart: 8, of which 8 were waited for; matrix products, arithmetic and copies ran while one was open for 2% of the time, Pallas kernels for 0%

commit v1 on v0

v1 whole, which is shorter than its diff:
```python
import functools
import jax
import jax.numpy as jnp
from jax import lax
from jax.experimental import pallas as pl
from jax.experimental.pallas import tpu as pltpu
from jax.sharding import PartitionSpec as P

epsilon = 1e-06
F32 = jnp.float32
BF16 = jnp.bfloat16
MESH = pl.DeviceIdType.MESH
NT = (((1,), (1,)), ((), ()))


def silu(a):
    return a / (1.0 + jnp.exp(-a))


def dot(a, b):
    return jnp.dot(a.astype(BF16), b.astype(BF16), preferred_element_type=F32)


def stack_kernel(
    stages,
    group,
    tokens,
    query_hbm,
    key_hbm,
    value_hbm,
    gate_hbm,
    strength,
    decay_in,
    decay_speed,
    spike,
    gain,
    closing_gain,
    out,
    weights,
    acc,
    xin,
    xout,
    yin,
    level,
    spike_columns,
    part_mine,
    part_other,
    w_sem,
    in_sem,
    entry_sem,
    fwd_send,
    fwd_recv,
    out_send,
    y_recv,
    part_send,
    part_recv,
):
    stage = lax.axis_index("pp")
    core = lax.axis_index("tp")
    last = stages - 1
    length, half = tokens.shape
    heads = xout.shape[1]
    width = half // heads
    model_width = group * half
    others = range(1, group)

    def peer(d):
        return lax.rem(core + d, group)

    loads = [
        pltpu.make_async_copy(ref, weights.at[i], w_sem.at[i])
        for i, ref in enumerate((query_hbm, key_hbm, value_hbm, gate_hbm))
    ]
    for load in loads:
        load.start()

    barrier = pltpu.get_barrier_semaphore()
    for d in range(1, stages):
        pl.semaphore_signal(
            barrier, inc=1, device_id={"pp": lax.rem(stage + d, stages)}, device_id_type=MESH
        )
    for d in others:
        pl.semaphore_signal(barrier, inc=1, device_id={"tp": peer(d)}, device_id_type=MESH)
    pl.semaphore_wait(barrier, stages + group - 2)

    def entry_copy(h):
        return pltpu.make_async_remote_copy(
            src_ref=xout.at[stages, h],
            dst_ref=xin.at[stage, core * heads + h],
            send_sem=entry_sem.at[h],
            recv_sem=in_sem.at[stage, h],
            device_id={"pp": 0},
            device_id_type=MESH,
        )

    def next_copy(m, h):
        return pltpu.make_async_remote_copy(
            src_ref=xout.at[m, h],
            dst_ref=xin.at[m, core * heads + h],
            send_sem=out_send.at[m, h],
            recv_sem=in_sem.at[m, h],
            device_id={"pp": lax.rem(stage + 1, stages)},
            device_id_type=MESH,
        )

    def exit_copy(m, h):
        return pltpu.make_async_remote_copy(
            src_ref=xout.at[m, h],
            dst_ref=yin.at[h],
            send_sem=out_send.at[m, h],
            recv_sem=y_recv.at[h],
            device_id={"pp": m},
            device_id_type=MESH,
        )

    def forward_copy(m, d, h):
        return pltpu.make_async_remote_copy(
            src_ref=xin.at[m, core * heads + h],
            dst_ref=xin.at[m, core * heads + h],
            send_sem=fwd_send.at[m, d - 1, h],
            recv_sem=fwd_recv.at[m, d - 1, h],
            device_id={"tp": peer(d)},
            device_id_type=MESH,
        )

    @pl.when(stage == 0)
    def _():
        for h in range(heads):
            xin[0, core * heads + h] = tokens[:, h * width : (h + 1) * width]

    @pl.when(stage > 0)
    def _():
        for h in range(heads):
            xout[stages, h] = tokens[:, h * width : (h + 1) * width]
        for h in range(heads):
            entry_copy(h).start()

    rows = lax.broadcasted_iota(jnp.int32, (length, length), 0)
    cols = lax.broadcasted_iota(jnp.int32, (length, length), 1)
    differ = rows ^ cols
    found = jnp.full((length, length), -1, jnp.int32)
    level_count = (length - 1).bit_length()
    for k in range(level_count):
        found = found + (differ >= (1 << k)).astype(jnp.int32)
    level[...] = jnp.where(rows > cols, found, jnp.where(rows == cols, -1, -2))

    spike_columns[...] = jnp.concatenate(
        [spike[...], jnp.zeros((length - heads, length), F32)], axis=0
    ).T

    def step(m, _):
        @pl.when((stage > 0) | (m > 0))
        def _():
            for h in range(heads):
                next_copy(m, h).wait_recv()
                for d in others:
                    forward_copy(m, d, h).start()

        @pl.when((stage == 0) & (m == 0))
        def _():
            for h in range(heads):
                for d in others:
                    forward_copy(m, d, h).start()

        @pl.when(m == 0)
        def _():
            for load in loads:
                load.wait()

        def gather(which):
            return jnp.concatenate([xin[m, which * heads + h] for h in range(heads)], axis=1)

        def project(x, which):
            own = pl.ds(pl.multiple_of(which * half, half), half)
            mats = [dot(x, weights[i, own, :]) for i in range(4)]
            small = [
                lax.dot_general(x, ref[:, own], NT, preferred_element_type=F32)
                for ref in (strength, decay_in)
            ]
            wide = x.astype(F32)
            return mats, small, jnp.sum(wide * wide, axis=1, keepdims=True)

        mats, small, squares = project(gather(core), core)
        for i in range(4):
            acc[i] = mats[i]
        for d in others:
            for h in range(heads):
                forward_copy(m, d, h).wait_recv()
            source = peer(group - d)
            mats, small_other, squares_other = project(gather(source), source)
            small = [a + b for a, b in zip(small, small_other)]
            squares = squares + squares_other
            if d < group - 1:
                for i in range(4):
                    acc[i] += mats[i]
        inv_rms = lax.rsqrt(squares / model_width + epsilon)
        beta = 1.0 / (1.0 + jnp.exp(-small[0] * inv_rms))
        pre = small[1][:, :heads] * inv_rms
        softplus = jnp.maximum(pre, 0.0) + jnp.log(1.0 + jnp.exp(-jnp.abs(pre)))
        log_decay = -decay_speed[...] * softplus + spike_columns[:, :heads]
        lev = level[...]
        lower = jnp.where(lev >= -1, 1.0, 0.0).astype(F32)
        padded = jnp.concatenate(
            [log_decay, jnp.zeros((length, length - heads), F32)], axis=1
        )
        cumulative = jnp.dot(
            lower, padded, precision=lax.Precision.HIGHEST, preferred_element_type=F32
        )
        cumulative_rows = cumulative.T
        every = range(heads)

        def columns(i, h):
            part = slice(h * width, (h + 1) * width)
            return (acc[i, :, part] + mats[i][:, part]) * inv_rms

        def unit(a):
            return a * lax.rsqrt(jnp.sum(a * a, axis=1, keepdims=True) + epsilon)

        keys = [unit(silu(columns(1, h))) for h in every]
        queries = [unit(silu(columns(0, h))) * width ** (-0.5) for h in every]
        gram = []
        for h in every:
            left = jnp.concatenate([keys[h] * beta[:, h : h + 1], queries[h]], axis=0)
            gram.append(
                lax.dot_general(
                    left.astype(BF16), keys[h].astype(BF16), NT, preferred_element_type=F32
                )
            )
        decayed = [
            jnp.exp(
                jnp.where(
                    lev >= -1, cumulative[:, h : h + 1] - cumulative_rows[h : h + 1, :], -jnp.inf
                )
            )
            for h in every
        ]
        system = [gram[h][:length] * decayed[h] for h in every]
        scores = [(gram[h][length:] * decayed[h]).astype(BF16) for h in every]

        def corner(h, k):
            return jnp.where(lev == k, system[h], 0.0).astype(BF16)

        eye = jnp.where(lev == -1, 1.0, 0.0).astype(F32)
        inverse = [eye - jnp.where(lev == 0, system[h], 0.0) for h in every]
        for k in range(1, level_count - 1):
            rounded = [inverse[h].astype(BF16) for h in every]
            partial = [dot(corner(h, k), rounded[h]) for h in every]
            inverse = [inverse[h] - dot(rounded[h], partial[h]) for h in every]
        rounded = [inverse[h].astype(BF16) for h in every]
        values = [silu(columns(2, h)) * beta[:, h : h + 1] for h in every]
        first = [dot(rounded[h], values[h]) for h in every]
        partial = [dot(corner(h, level_count - 1), first[h]) for h in every]
        update = [first[h] - dot(rounded[h], partial[h]) for h in every]
        mixed = [dot(scores[h], update[h]) for h in every]
        for h in every:
            gate = silu(columns(3, h))
            scale = lax.rsqrt(jnp.mean(mixed[h] * mixed[h], axis=1, keepdims=True) + epsilon)
            head_out = mixed[h] * scale * gain[:, h * width : (h + 1) * width] * gate
            before = xin[m, core * heads + h].astype(F32)
            xout[m, h] = (before + head_out.astype(BF16).astype(F32)).astype(BF16)

        @pl.when(stage < last)
        def _():
            for h in range(heads):
                next_copy(m, h).start()

        @pl.when((stage == last) & (m < last))
        def _():
            for h in range(heads):
                exit_copy(m, h).start()

        return 0

    lax.fori_loop(0, stages, step, 0)

    @pl.when(stage == last)
    def _():
        for h in range(heads):
            yin[h] = xout[last, h]

    @pl.when(stage < last)
    def _():
        for h in range(heads):
            exit_copy(0, h).wait_recv()

    final = [yin[h].astype(F32) for h in range(heads)]
    total = sum(jnp.sum(a * a, axis=1, keepdims=True) for a in final)
    part_mine[...] = jnp.broadcast_to(total, part_mine.shape)
    part_copies = [
        pltpu.make_async_remote_copy(
            src_ref=part_mine,
            dst_ref=part_other.at[d - 1],
            send_sem=part_send.at[d - 1],
            recv_sem=part_recv.at[d - 1],
            device_id={"tp": peer(d)},
            device_id_type=MESH,
        )
        for d in others
    ]
    for copy in part_copies:
        copy.start()

    @pl.when(stage > 0)
    def _():
        for h in range(heads):
            entry_copy(h).wait_send()

    def drain(m, _):
        for h in range(heads):
            for d in others:
                forward_copy(m, d, h).wait_send()

        @pl.when((stage < last) | (m < last))
        def _():
            for h in range(heads):
                next_copy(m, h).wait_send()

        return 0

    lax.fori_loop(0, stages, drain, 0)
    total = part_mine[...]
    for copy in part_copies:
        copy.wait()
    for d in others:
        total = total + part_other[d - 1]
    inv_rms = lax.rsqrt(total / model_width + epsilon)
    for h in range(heads):
        part = slice(h * width, (h + 1) * width)
        out[:, part] = (final[h] * inv_rms * closing_gain[:, part]).astype(BF16)


def on_device(
    stages,
    group,
    tokens,
    query_matrix,
    key_matrix,
    value_matrix,
    output_gate_weight,
    strength_weight,
    decay_input_weight,
    decay_scale_table,
    log_spike_decay,
    head_norm_gain,
    closing_norm_gain,
):
    _, length, half = tokens.shape
    heads = strength_weight.shape[-1]
    width = half // heads

    def rows_of(weight):
        return jnp.pad(weight[0].T, ((0, 1), (0, 0))) if heads == 1 else weight[0].T

    vmem = pl.BlockSpec(memory_space=pltpu.VMEM)
    anywhere = pl.BlockSpec(memory_space=pl.ANY)
    dma = pltpu.SemaphoreType.DMA
    result = pl.pallas_call(
        functools.partial(stack_kernel, stages, group),
        out_shape=jax.ShapeDtypeStruct((length, half), BF16),
        in_specs=[vmem] + [anywhere] * 4 + [vmem] * 6,
        out_specs=vmem,
        scratch_shapes=[
            pltpu.VMEM((4, group * half, half), BF16),
            pltpu.VMEM((4, length, half), F32),
            pltpu.VMEM((stages, group * heads, length, width), BF16),
            pltpu.VMEM((stages + 1, heads, length, width), BF16),
            pltpu.VMEM((heads, length, width), BF16),
            pltpu.VMEM((length, length), jnp.int32),
            pltpu.VMEM((length, length), F32),
            pltpu.VMEM((length, width), F32),
            pltpu.VMEM((group - 1, length, width), F32),
            dma((4,)),
            dma((stages, heads)),
            dma((heads,)),
            dma((stages, group - 1, heads)),
            dma((stages, group - 1, heads)),
            dma((stages, heads)),
            dma((heads,)),
            dma((group - 1,)),
            dma((group - 1,)),
        ],
        compiler_params=pltpu.CompilerParams(
            collective_id=0, has_side_effects=True, vmem_limit_bytes=60 * 1024 * 1024
        ),
    )(
        tokens[0],
        query_matrix[0],
        key_matrix[0],
        value_matrix[0],
        output_gate_weight[0],
        rows_of(strength_weight),
        rows_of(decay_input_weight),
        decay_scale_table,
        log_spike_decay[0].T,
        head_norm_gain,
        closing_norm_gain[None],
    )
    return result[None]


def solution(mesh):
    placed = (
        P("pp", "fs", "tp"),
        P("pp", None, "tp"),
        P("pp", None, "tp"),
        P("pp", None, "tp"),
        P("pp", None, "tp"),
        P("pp", None, "tp"),
        P("pp", None, "tp"),
        P("pp", "tp"),
        P("pp", None, "tp"),
        P("pp", "tp"),
        P("tp"),
    )
    return jax.shard_map(
        functools.partial(on_device, mesh.shape["pp"], mesh.shape["tp"]),
        mesh=mesh,
        in_specs=placed,
        out_specs=P("pp", "fs", "tp"),
        check_vma=False,
    )
```

time: 536 us -> 57.3 us (0.11)
  the two profiles are of different devices: /device:TPU:0 before, /device:TPU:19 now
where the time goes in v1:
time: 57.3 us; the launch traced here: 57.2 us
  Pallas kernels  55.6 us (97%)
  local copies, waits for them, and re-layouts  1.57 us (3%)
    pallas_call x1, Pallas kernels, on_device(): pl.pallas_call(functools.partial(stack_kernel, stages, group), out_shape=...  55.6 us
    unnamed x1, local copies, waits for them, and re-layouts  1.57 us

profile of v1, /device:TPU:19, one launch (start us, length us, event | category | flops | bytes accessed | tf_op | source)
XLA Modules:
  0.0 57.2 jit_solution(6627099539598147567)
XLA Ops:
  0.0 55.6 %shard_map.109 = bf16[128,512]{1,0:T(8,128)(2,1)} custom-call(bf16[128,512]{1,0:T(8,128)(2,1)} %bitcast.21, bf16[1024,512]{1,0:T(8,128)(2,1)} %bitcast.16, bf16[1024,512]{1,0:T(8,128)(2,1)} %bitcast.17, bf16[1024,512]{1,0:T(8,128)(2,1)} %bitcast.18, bf16[1024,512]{1,0:T(8,128)(2,1)} %bitcast.19, bf16[4,1024]{1,0:T(4,128)(2,1)} %bitcast.22, ...), custom_call_target="tpu_custom_call" | custom-call | tf_op jit(solution)/shard_map/pallas_call | solution.py:357
  55.6 1.6 %copy.13 = bf16[1,128,512]{2,1,0:T(8,128)(2,1)} copy(bf16[1,128,512]{2,1,0:T(8,128)(2,1)} %bitcast.20) | data formatting | bytes 262144

commit v2 on v1

--- a/solution.py
+++ b/solution.py
@@ -29,13 +29,19 @@
     key_hbm,
     value_hbm,
     gate_hbm,
+    strength_hbm,
+    decay_in_hbm,
+    decay_speed_hbm,
+    spike_hbm,
+    gain_hbm,
+    closing_hbm,
+    out,
     strength,
     decay_in,
     decay_speed,
     spike,
     gain,
     closing_gain,
-    out,
     weights,
     acc,
     xin,
@@ -46,6 +52,9 @@
     part_mine,
     part_other,
     w_sem,
+    small_sem,
+    token_sem,
+    go_sem,
     in_sem,
     entry_sem,
     fwd_send,
@@ -67,6 +76,44 @@
     def peer(d):
         return lax.rem(core + d, group)
 
+    barrier = pltpu.get_barrier_semaphore()
+    for d in range(1, stages):
+        pl.semaphore_signal(
+            barrier, inc=1, device_id={"pp": lax.rem(stage + d, stages)}, device_id_type=MESH
+        )
+    for d in others:
+        pl.semaphore_signal(barrier, inc=1, device_id={"tp": peer(d)}, device_id_type=MESH)
+
+    def token_copy(h, target):
+        return pltpu.make_async_copy(
+            tokens.at[:, h * width : (h + 1) * width], target, token_sem.at[h]
+        )
+
+    @pl.when(stage == 0)
+    def _():
+        for h in range(heads):
+            token_copy(h, xin.at[0, core * heads + h]).start()
+
+    @pl.when(stage > 0)
+    def _():
+        for h in range(heads):
+            token_copy(h, xout.at[stages, h]).start()
+
+    small_loads = [
+        pltpu.make_async_copy(a, b, small_sem.at[i])
+        for i, (a, b) in enumerate(
+            (
+                (strength_hbm, strength),
+                (decay_in_hbm, decay_in),
+                (decay_speed_hbm, decay_speed),
+                (spike_hbm, spike),
+                (gain_hbm, gain),
+                (closing_hbm, closing_gain),
+            )
+        )
+    ]
+    for load in small_loads:
+        load.start()
     loads = [
         pltpu.make_async_copy(ref, weights.at[i], w_sem.at[i])
         for i, ref in enumerate((query_hbm, key_hbm, value_hbm, gate_hbm))
@@ -74,13 +121,6 @@
     for load in loads:
         load.start()
 
-    barrier = pltpu.get_barrier_semaphore()
-    for d in range(1, stages):
-        pl.semaphore_signal(
-            barrier, inc=1, device_id={"pp": lax.rem(stage + d, stages)}, device_id_type=MESH
-        )
-    for d in others:
-        pl.semaphore_signal(barrier, inc=1, device_id={"tp": peer(d)}, device_id_type=MESH)
     pl.semaphore_wait(barrier, stages + group - 2)
 
     def entry_copy(h):
@@ -126,14 +166,28 @@
     @pl.when(stage == 0)
     def _():
         for h in range(heads):
-            xin[0, core * heads + h] = tokens[:, h * width : (h + 1) * width]
+            token_copy(h, xin.at[0, core * heads + h]).wait()
+
+    early = max(heads - 2, 0)
 
     @pl.when(stage > 0)
     def _():
         for h in range(heads):
-            xout[stages, h] = tokens[:, h * width : (h + 1) * width]
+            token_copy(h, xout.at[stages, h]).wait()
+
+        @pl.when(stage > 1)
+        def _():
+            pl.semaphore_wait(go_sem, 1)
+
         for h in range(heads):
             entry_copy(h).start()
+        entry_copy(early).wait_send()
+
+        @pl.when(stage < last)
+        def _():
+            pl.semaphore_signal(
+                go_sem, inc=1, device_id={"pp": lax.rem(stage + 1, stages)}, device_id_type=MESH
+            )
 
     rows = lax.broadcasted_iota(jnp.int32, (length, length), 0)
     cols = lax.broadcasted_iota(jnp.int32, (length, length), 1)
@@ -144,6 +198,8 @@
         found = found + (differ >= (1 << k)).astype(jnp.int32)
     level[...] = jnp.where(rows > cols, found, jnp.where(rows == cols, -1, -2))
 
+    for load in small_loads:
+        load.wait()
     spike_columns[...] = jnp.concatenate(
         [spike[...], jnp.zeros((length - heads, length), F32)], axis=0
     ).T
@@ -303,7 +359,8 @@
     @pl.when(stage > 0)
     def _():
         for h in range(heads):
-            entry_copy(h).wait_send()
+            if h != early:
+                entry_copy(h).wait_send()
 
     def drain(m, _):
         for h in range(heads):
@@ -352,14 +409,20 @@
         return jnp.pad(weight[0].T, ((0, 1), (0, 0))) if heads == 1 else weight[0].T
 
     vmem = pl.BlockSpec(memory_space=pltpu.VMEM)
-    anywhere = pl.BlockSpec(memory_space=pl.ANY)
+    anywhere = pl.BlockSpec(memory_space=pltpu.HBM)
     dma = pltpu.SemaphoreType.DMA
     result = pl.pallas_call(
         functools.partial(stack_kernel, stages, group),
-        out_shape=jax.ShapeDtypeStruct((length, half), BF16),
-        in_specs=[vmem] + [anywhere] * 4 + [vmem] * 6,
+        out_shape=pltpu.VMEM((length, half), BF16),
+        in_specs=[anywhere] * 11,
         out_specs=vmem,
         scratch_shapes=[
+            pltpu.VMEM((max(heads, 2), group * half), BF16),
+            pltpu.VMEM((max(heads, 2), group * half), BF16),
+            pltpu.VMEM((1, heads), F32),
+            pltpu.VMEM((heads, length), F32),
+            pltpu.VMEM((1, half), F32),
+            pltpu.VMEM((1, half), F32),
             pltpu.VMEM((4, group * half, half), BF16),
             pltpu.VMEM((4, length, half), F32),
             pltpu.VMEM((stages, group * heads, length, width), BF16),
@@ -370,6 +433,9 @@
             pltpu.VMEM((length, width), F32),
             pltpu.VMEM((group - 1, length, width), F32),
             dma((4,)),
+            dma((6,)),
+            dma((heads,)),
+            pltpu.SemaphoreType.REGULAR,
             dma((stages, heads)),
             dma((heads,)),
             dma((stages, group - 1, heads)),

time: 57.3 us -> 50 us (0.87)
  Pallas kernels: 55.6 us -> 49.1 us
  local copies, waits for them, and re-layouts: 1.57 us -> 0.66 us
    pallas_call x1, Pallas kernels: 55.6 us -> 49.1 us  [on_device(): pl.pallas_call(functools.partial(stack_kernel, stages, group), out_shape=...]
    unnamed x1, local copies, waits for them, and re-layouts: 1.57 us -> 0.66 us
where the time goes in v2:
time: 50 us; the launch traced here: 49.8 us
  Pallas kernels  49.1 us (98%)
  local copies, waits for them, and re-layouts  0.66 us (1%)
    pallas_call x1, Pallas kernels, on_device(): pl.pallas_call(functools.partial(stack_kernel, stages, group), out_shape=...  49.1 us

profile of v2, /device:TPU:19, one launch (start us, length us, event | category | flops | bytes accessed | tf_op | source)
XLA Modules:
  0.0 49.8 jit_solution(1848489744918449070)
XLA Ops:
  0.0 49.1 %shard_map.109 = bf16[128,512]{1,0:T(8,128)(2,1)S(1)} custom-call(bf16[128,512]{1,0:T(8,128)(2,1)} %bitcast.21, bf16[1024,512]{1,0:T(8,128)(2,1)} %bitcast.17, bf16[1024,512]{1,0:T(8,128)(2,1)} %bitcast.18, bf16[1024,512]{1,0:T(8,128)(2,1)} %bitcast.19, bf16[1024,512]{1,0:T(8,128)(2,1)} %bitcast.20, bf16[4,1024]{1,0:T(4,128)(2,1)} %bitcast.22, ...), custom_call_target="tpu_custom_call" | custom-call | tf_op jit(solution)/shard_map/pallas_call | solution.py:414
  49.2 0.7 %copy.13 = bf16[1,128,512]{2,1,0:T(8,128)(2,1)} copy(bf16[1,128,512]{2,1,0:T(8,128)(2,1)S(1)} %bitcast.16) | data formatting | bytes 262144

commit v3 on v2

--- a/solution.py
+++ b/solution.py
@@ -204,6 +204,71 @@
         [spike[...], jnp.zeros((length - heads, length), F32)], axis=0
     ).T
 
+    def finish(m, every, part, source, inv_rms, beta, cumulative, cumulative_rows):
+        own = pl.ds(pl.multiple_of(source * half, half), half)
+        wanted = slice(every[0] * width, (every[-1] + 1) * width)
+        mats = [dot(part, weights[i, own, wanted]) for i in range(4)]
+        lev = level[...]
+
+        def columns(i, h):
+            at = (h - every[0]) * width
+            before = acc[i, :, h * width : (h + 1) * width]
+            return (before + mats[i][:, at : at + width]) * inv_rms
+
+        def unit(a):
+            return a * lax.rsqrt(jnp.sum(a * a, axis=1, keepdims=True) + epsilon)
+
+        keys = {h: unit(silu(columns(1, h))) for h in every}
+        queries = {h: unit(silu(columns(0, h))) * width ** (-0.5) for h in every}
+        gram = {}
+        for h in every:
+            left = jnp.concatenate([keys[h] * beta[:, h : h + 1], queries[h]], axis=0)
+            gram[h] = lax.dot_general(
+                left.astype(BF16), keys[h].astype(BF16), NT, preferred_element_type=F32
+            )
+        decayed = {
+            h: jnp.exp(
+                jnp.where(
+                    lev >= -1, cumulative[:, h : h + 1] - cumulative_rows[h : h + 1, :], -jnp.inf
+                )
+            )
+            for h in every
+        }
+        system = {h: gram[h][:length] * decayed[h] for h in every}
+        scores = {h: (gram[h][length:] * decayed[h]).astype(BF16) for h in every}
+
+        def corner(h, k):
+            return jnp.where(lev == k, system[h], 0.0).astype(BF16)
+
+        eye = jnp.where(lev == -1, 1.0, 0.0).astype(F32)
+        inverse = {h: eye - jnp.where(lev == 0, system[h], 0.0) for h in every}
+        for k in range(1, level_count - 1):
+            rounded = {h: inverse[h].astype(BF16) for h in every}
+            partial = {h: dot(corner(h, k), rounded[h]) for h in every}
+            inverse = {h: inverse[h] - dot(rounded[h], partial[h]) for h in every}
+        rounded = {h: inverse[h].astype(BF16) for h in every}
+        values = {h: silu(columns(2, h)) * beta[:, h : h + 1] for h in every}
+        first = {h: dot(rounded[h], values[h]) for h in every}
+        partial = {h: dot(corner(h, level_count - 1), first[h]) for h in every}
+        update = {h: first[h] - dot(rounded[h], partial[h]) for h in every}
+        mixed = {h: dot(scores[h], update[h]) for h in every}
+        for h in every:
+            gate = silu(columns(3, h))
+            scale = lax.rsqrt(jnp.mean(mixed[h] * mixed[h], axis=1, keepdims=True) + epsilon)
+            head_out = mixed[h] * scale * gain[:, h * width : (h + 1) * width] * gate
+            before = xin[m, core * heads + h].astype(F32)
+            xout[m, h] = (before + head_out.astype(BF16).astype(F32)).astype(BF16)
+
+        @pl.when(stage < last)
+        def _():
+            for h in every:
+                next_copy(m, h).start()
+
+        @pl.when((stage == last) & (m < last))
+        def _():
+            for h in every:
+                exit_copy(m, h).start()
+
     def step(m, _):
         @pl.when((stage > 0) | (m > 0))
         def _():
@@ -226,29 +291,32 @@
         def gather(which):
             return jnp.concatenate([xin[m, which * heads + h] for h in range(heads)], axis=1)
 
+        def rows_from(which):
+            return pl.ds(pl.multiple_of(which * half, half), half)
+
         def project(x, which):
-            own = pl.ds(pl.multiple_of(which * half, half), half)
-            mats = [dot(x, weights[i, own, :]) for i in range(4)]
             small = [
-                lax.dot_general(x, ref[:, own], NT, preferred_element_type=F32)
+                lax.dot_general(x, ref[:, rows_from(which)], NT, preferred_element_type=F32)
                 for ref in (strength, decay_in)
             ]
             wide = x.astype(F32)
-            return mats, small, jnp.sum(wide * wide, axis=1, keepdims=True)
-
-        mats, small, squares = project(gather(core), core)
+            return small, jnp.sum(wide * wide, axis=1, keepdims=True)
+
+        own_part = gather(core)
+        small, squares = project(own_part, core)
         for i in range(4):
-            acc[i] = mats[i]
+            acc[i] = dot(own_part, weights[i, rows_from(core), :])
         for d in others:
             for h in range(heads):
                 forward_copy(m, d, h).wait_recv()
             source = peer(group - d)
-            mats, small_other, squares_other = project(gather(source), source)
+            part = gather(source)
+            small_other, squares_other = project(part, source)
             small = [a + b for a, b in zip(small, small_other)]
             squares = squares + squares_other
             if d < group - 1:
                 for i in range(4):
-                    acc[i] += mats[i]
+                    acc[i] += dot(part, weights[i, rows_from(source), :])
         inv_rms = lax.rsqrt(squares / model_width + epsilon)
         beta = 1.0 / (1.0 + jnp.exp(-small[0] * inv_rms))
         pre = small[1][:, :heads] * inv_rms
@@ -263,67 +331,10 @@
             lower, padded, precision=lax.Precision.HIGHEST, preferred_element_type=F32
         )
         cumulative_rows = cumulative.T
-        every = range(heads)
-
-        def columns(i, h):
-            part = slice(h * width, (h + 1) * width)
-            return (acc[i, :, part] + mats[i][:, part]) * inv_rms
-
-        def unit(a):
-            return a * lax.rsqrt(jnp.sum(a * a, axis=1, keepdims=True) + epsilon)
-
-        keys = [unit(silu(columns(1, h))) for h in every]
-        queries = [unit(silu(columns(0, h))) * width ** (-0.5) for h in every]
-        gram = []
-        for h in every:
-            left = jnp.concatenate([keys[h] * beta[:, h : h + 1], queries[h]], axis=0)
-            gram.append(
-                lax.dot_general(
-                    left.astype(BF16), keys[h].astype(BF16), NT, preferred_element_type=F32
-                )
-            )
-        decayed = [
-            jnp.exp(
-                jnp.where(
-                    lev >= -1, cumulative[:, h : h + 1] - cumulative_rows[h : h + 1, :], -jnp.inf
-                )
-            )
-            for h in every
-        ]
-        system = [gram[h][:length] * decayed[h] for h in every]
-        scores = [(gram[h][length:] * decayed[h]).astype(BF16) for h in every]
-
-        def corner(h, k):
-            return jnp.where(lev == k, system[h], 0.0).astype(BF16)
-
-        eye = jnp.where(lev == -1, 1.0, 0.0).astype(F32)
-        inverse = [eye - jnp.where(lev == 0, system[h], 0.0) for h in every]
-        for k in range(1, level_count - 1):
-            rounded = [inverse[h].astype(BF16) for h in every]
-            partial = [dot(corner(h, k), rounded[h]) for h in every]
-            inverse = [inverse[h] - dot(rounded[h], partial[h]) for h in every]
-        rounded = [inverse[h].astype(BF16) for h in every]
-        values = [silu(columns(2, h)) * beta[:, h : h + 1] for h in every]
-        first = [dot(rounded[h], values[h]) for h in every]
-        partial = [dot(corner(h, level_count - 1), first[h]) for h in every]
-        update = [first[h] - dot(rounded[h], partial[h]) for h in every]
-        mixed = [dot(scores[h], update[h]) for h in every]
-        for h in every:
-            gate = silu(columns(3, h))
-            scale = lax.rsqrt(jnp.mean(mixed[h] * mixed[h], axis=1, keepdims=True) + epsilon)
-            head_out = mixed[h] * scale * gain[:, h * width : (h + 1) * width] * gate
-            before = xin[m, core * heads + h].astype(F32)
-            xout[m, h] = (before + head_out.astype(BF16).astype(F32)).astype(BF16)
-
-        @pl.when(stage < last)
-        def _():
-            for h in range(heads):
-                next_copy(m, h).start()
-
-        @pl.when((stage == last) & (m < last))
-        def _():
-            for h in range(heads):
-                exit_copy(m, h).start()
+        pair = max(heads // 2, 1)
+        for every in [range(a, a + pair) for a in range(0, heads, pair)]:
+            finish(m, every, part, source, inv_rms, beta, cumulative, cumulative_rows)
+
 
         return 0
 

time: 50 us -> 61.8 us (1.24)
  the two profiles are of different devices: /device:TPU:19 before, /device:TPU:25 now
where the time goes in v3:
time: 61.8 us; the launch traced here: 61.7 us
  Pallas kernels  61 us (99%)
  local copies, waits for them, and re-layouts  0.66 us (1%)
    pallas_call x1, Pallas kernels, on_device(): pl.pallas_call(functools.partial(stack_kernel, stages, group), out_shape=...  61 us

profile of v3, /device:TPU:25, one launch (start us, length us, event | category | flops | bytes accessed | tf_op | source)
XLA Modules:
  0.0 61.7 jit_solution(456771835804079356)
XLA Ops:
  0.0 61.0 %shard_map.109 = bf16[128,512]{1,0:T(8,128)(2,1)S(1)} custom-call(bf16[128,512]{1,0:T(8,128)(2,1)} %bitcast.21, bf16[1024,512]{1,0:T(8,128)(2,1)} %bitcast.17, bf16[1024,512]{1,0:T(8,128)(2,1)} %bitcast.18, bf16[1024,512]{1,0:T(8,128)(2,1)} %bitcast.19, bf16[1024,512]{1,0:T(8,128)(2,1)} %bitcast.20, bf16[4,1024]{1,0:T(4,128)(2,1)} %bitcast.22, ...), custom_call_target="tpu_custom_call" | custom-call | tf_op jit(solution)/shard_map/pallas_call | solution.py:425
  61.0 0.7 %copy.13 = bf16[1,128,512]{2,1,0:T(8,128)(2,1)} copy(bf16[1,128,512]{2,1,0:T(8,128)(2,1)S(1)} %bitcast.16) | data formatting | bytes 262144
